TPU v7x, 128 devices: a whole 4x4x4 slice. The times are simulated.
128 devices in a mesh: ep: 128 (over z, y, x, core).
Axes of the slice: x: 4, y: 4, z: 4, core: 2. Of those that a mesh axis runs over, the one named last changes fastest.
Arguments:
- hidden_in: bfloat16 [256, 2048], P('ep'), may hold values from -6 to 6
- lengths: int32 [256], P('ep'), may hold values from 1 to 1024, as said below
- key_cache: bfloat16 [256, 1024, 512], P('ep'), may hold values from -30 to 30
- value_cache: bfloat16 [256, 1024, 512], P('ep'), may hold values from -6 to 6
- query_w: bfloat16 [2048, 2048], P('ep'), may hold values from -0.125 to 0.125
- key_w: bfloat16 [2048, 512], P('ep'), may hold values from -0.125 to 0.125
- value_w: bfloat16 [2048, 512], P('ep'), may hold values from -0.125 to 0.125
- out_w: bfloat16 [2048, 2048], P('ep'), may hold values from -0.125 to 0.125
- lam_heads: float32 [8], replicated, may hold values from 0.3 to 0.8
- head_gain: float32 [256], replicated, may hold values from 0.1 to 1.9
- attn_gain: float32 [2048], replicated, may hold values from 0.1 to 1.9
- moe_gain: float32 [2048], replicated, may hold values from 0.1 to 1.9
- routing: int32 [256, 6], replicated, may hold values from 0 to 127, all different within a row; in each aligned block of 256 rows (0 to 255, 256 to 511, ...) at most 24 rows name the same one
- route_weight: float32 [256, 6], replicated, may hold values from 0.1 to 0.6
- gate_w: bfloat16 [128, 2048, 512], P('ep'), may hold values from -0.125 to 0.125
- up_w: bfloat16 [128, 2048, 512], P('ep'), may hold values from -0.125 to 0.125
- down_w: bfloat16 [128, 512, 2048], P('ep'), may hold values from -0.25 to 0.25
- shared_gate: bfloat16 [2048, 512], replicated, may hold values from -0.125 to 0.125
- shared_up: bfloat16 [2048, 512], replicated, may hold values from -0.125 to 0.125
- shared_down: bfloat16 [512, 2048], replicated, may hold values from -0.25 to 0.25
Outputs:
- layer_out: bfloat16 [256, 2048], P('ep')
- key_new: bfloat16 [256, 512], P('ep')
- value_new: bfloat16 [256, 512], P('ep')
Inputs may be any that keep to these rules, and one draw needn't show every extreme that they name: `lengths`: some sequence has exactly 1024 positions in use. `routing`: each row names 6 different experts; no expert is named by more than 24 rows, a bound that some block reaches.
All inputs are finite; a program needn't handle non-finite values.
Results may differ from a plain program's by a relative error of at most 0.013.
The roundings to bfloat16 on the way count: a program that leaves them out, or rounds other values in their place, can miss the bound.
Values may be sent and summed in bfloat16 or wider, within the bound.
No kernel may reach another device: no remote copies, remote signals or barrier semaphores. Data moves between devices by JAX's collectives and lax.ppermute only.
A program may use at most 64 MiB of HBM per device.

v0:
```python
import jax
import jax.numpy as jnp
from jax import lax
from jax.sharding import Mesh
from jax.sharding import PartitionSpec as P

KV_HEADS = 2
HEAD_DIM = 128
EXP_CAP = 24
EP = ("ep_0", "ep_1", "ep_2", "ep_3")
eps_norm = 1e-06
eps_head = 1e-05
theta_base = 500000.0


def split_up(value, dim, length):
    dims = value.shape
    blocks = value.reshape(*dims[:dim], length, dims[dim] // length, *dims[dim + 1 :])
    return jnp.moveaxis(blocks, dim, 0)


def sent_and_summed(value, axis, dim):
    blocks = split_up(value, dim, lax.axis_size(axis))
    arrived = lax.all_to_all(blocks, axis, split_axis=0, concat_axis=0, tiled=True)
    return arrived.astype(jnp.float32).sum(axis=0)


def summed_rows(value, axes, dim):
    far, near = axes
    blocks = split_up(value, dim, lax.axis_size(far))
    nearer = sent_and_summed(blocks, near, dim + 1)
    arrived = lax.all_to_all(
        nearer.astype(jnp.bfloat16), far, split_axis=0, concat_axis=0, tiled=True
    )
    return arrived.astype(jnp.float32).sum(axis=0)


def rms_scale(row_block, gain_vec, epsilon):
    row_block = row_block.astype(jnp.float32)
    return (
        row_block
        * lax.rsqrt(jnp.mean(row_block * row_block, axis=-1, keepdims=True) + epsilon)
        * gain_vec
    )


def rotate(vectors, positions):
    half_width = vectors.shape[-1] // 2
    inverse = theta_base ** (-jnp.arange(half_width, dtype=jnp.float32) / half_width)
    angles = positions.astype(jnp.float32)[..., None] * inverse
    cosine, sine_part = (jnp.cos(angles), jnp.sin(angles))
    lower_half, upper_half = (vectors[..., :half_width], vectors[..., half_width:])
    return jnp.concatenate(
        [
            lower_half * cosine - upper_half * sine_part,
            lower_half * sine_part + upper_half * cosine,
        ],
        axis=-1,
    )


def attend(queries, key_new, value_new, cache_keys, cache_values, lengths, lam_heads, head_gain):
    num_seqs, kv_heads, group_size = (queries.shape[0], queries.shape[1], queries.shape[2])
    head_dim = queries.shape[-1]
    cache_len = cache_keys.shape[1]
    cache_keys = cache_keys.reshape(num_seqs, cache_len, kv_heads, 2, head_dim)
    cache_values = cache_values.reshape(num_seqs, cache_len, kv_heads, -1)
    value_new = value_new.reshape(num_seqs, kv_heads, -1)
    score_scale = head_dim ** (-0.5)
    scores = (
        jnp.einsum("skgph,sckph->skgpc", queries, cache_keys, preferred_element_type=jnp.float32)
        * score_scale
    )
    self_score = (
        jnp.einsum("skgph,skph->skgp", queries, key_new, preferred_element_type=jnp.float32)
        * score_scale
    )
    live_mask = (jnp.arange(cache_len)[None, :] < lengths[:, None])[:, None, None, None, :]
    peak = jnp.maximum(jnp.max(jnp.where(live_mask, scores, -jnp.inf), axis=-1), self_score)
    weights = jnp.where(live_mask, jnp.exp(scores - peak[..., None]), 0.0)
    self_weight = jnp.exp(self_score - peak)
    totals = jnp.sum(weights, axis=-1) + self_weight
    lambda_grid = lam_heads.reshape(kv_heads, group_size)[None]
    combined = (
        weights[:, :, :, 0] / totals[:, :, :, 0, None]
        - lambda_grid[..., None] * weights[:, :, :, 1] / totals[:, :, :, 1, None]
    ).astype(jnp.bfloat16)
    self_combined = (
        self_weight[..., 0] / totals[..., 0] - lambda_grid * self_weight[..., 1] / totals[..., 1]
    ).astype(jnp.bfloat16)
    head_out = jnp.einsum(
        "skgc,sckv->skgv", combined, cache_values, preferred_element_type=jnp.float32
    )
    head_out = (
        head_out
        + self_combined.astype(jnp.float32)[..., None]
        * value_new.astype(jnp.float32)[:, :, None, :]
    )
    return rms_scale(head_out, head_gain, eps_head).astype(jnp.bfloat16).reshape(num_seqs, -1)


def expert_rows(row_block, routed_here, gate_one, up_one, down_one):
    slot_index = jnp.cumsum(routed_here) - 1
    pick_table = (
        (slot_index[None, :] == jnp.arange(EXP_CAP)[:, None]) & (routed_here[None, :] > 0)
    ).astype(jnp.bfloat16)
    picked = jnp.dot(pick_table, row_block, preferred_element_type=jnp.float32).astype(jnp.bfloat16)
    hidden = (
        jax.nn.silu(jnp.dot(picked, gate_one, preferred_element_type=jnp.float32))
        * jnp.dot(picked, up_one, preferred_element_type=jnp.float32)
    ).astype(jnp.bfloat16)
    result = jnp.dot(hidden, down_one, preferred_element_type=jnp.float32).astype(jnp.bfloat16)
    return jnp.dot(pick_table.T, result, preferred_element_type=jnp.float32)


def on_device(
    hidden_in,
    lengths,
    key_cache,
    value_cache,
    query_w,
    key_w,
    value_w,
    out_w,
    lam_heads,
    head_gain,
    attn_gain,
    moe_gain,
    routing,
    route_weight,
    gate_w,
    up_w,
    down_w,
    shared_gate,
    shared_up,
    shared_down,
):
    devices = lax.axis_size(EP)
    device = lax.axis_index(EP)
    tok_dev = hidden_in.shape[0]
    model_width = hidden_in.shape[1]
    all_rows = lax.all_gather(hidden_in, EP, axis=0, tiled=True)
    normed = rms_scale(all_rows, attn_gain, eps_norm).astype(jnp.bfloat16)
    joined_rows = jnp.concatenate([query_w, key_w, value_w], axis=1)
    column_block = lax.all_to_all(joined_rows, EP, split_axis=1, concat_axis=0, tiled=True)
    column_sums = jnp.dot(normed, column_block, preferred_element_type=jnp.float32)
    projected = lax.all_to_all(column_sums, EP, split_axis=0, concat_axis=1, tiled=True)
    query_cols = query_w.shape[1]
    key_cols = key_w.shape[1]
    queries = rotate(
        projected[:, :query_cols].reshape(tok_dev, KV_HEADS, -1, 2, HEAD_DIM),
        lengths[:, None, None, None],
    ).astype(jnp.bfloat16)
    key_new = rotate(
        projected[:, query_cols : query_cols + key_cols].reshape(tok_dev, KV_HEADS, 2, HEAD_DIM),
        lengths[:, None, None],
    ).astype(jnp.bfloat16)
    value_new = projected[:, query_cols + key_cols :].astype(jnp.bfloat16)
    attn_out = attend(
        queries, key_new, value_new, key_cache, value_cache, lengths, lam_heads, head_gain
    )
    pieces = lax.all_to_all(attn_out, EP, split_axis=1, concat_axis=0, tiled=True)
    routed_here = jnp.sum((routing == device).astype(jnp.int32), axis=1)
    attn_proj = summed_rows(
        jnp.dot(pieces, out_w, preferred_element_type=jnp.float32).astype(jnp.bfloat16),
        (("ep_0", "ep_1", "ep_2"), "ep_3"),
        0,
    ).astype(jnp.bfloat16)
    after_mixer = (hidden_in.astype(jnp.float32) + attn_proj.astype(jnp.float32)).astype(
        jnp.bfloat16
    )
    moe_in = rms_scale(after_mixer, moe_gain, eps_norm).astype(jnp.bfloat16)
    own_routes = lax.dynamic_slice_in_dim(routing, device * tok_dev, tok_dev, 0)
    own_weights = lax.dynamic_slice_in_dim(route_weight, device * tok_dev, tok_dev, 0)
    expert_ids = jnp.arange(devices, dtype=jnp.int32)
    matches = own_routes[:, :, None] == expert_ids[None, None, :]
    chosen = jnp.any(matches, axis=1)
    weight_grid = jnp.sum(jnp.where(matches, own_weights[:, :, None], 0.0), axis=1)
    outgoing = jnp.where(chosen.T[:, :, None], moe_in[None], jnp.zeros((), jnp.bfloat16))
    arrived = lax.all_to_all(outgoing, EP, split_axis=0, concat_axis=0, tiled=True)
    result = expert_rows(
        arrived.reshape(devices * tok_dev, model_width), routed_here, gate_w[0], up_w[0], down_w[0]
    ).astype(jnp.bfloat16)
    returned = lax.all_to_all(
        result.reshape(devices, tok_dev, model_width), EP, split_axis=0, concat_axis=0, tiled=True
    )
    routed = jnp.sum(returned.astype(jnp.float32) * weight_grid.T[:, :, None], axis=0)
    shared_hidden = (
        jax.nn.silu(jnp.dot(moe_in, shared_gate, preferred_element_type=jnp.float32))
        * jnp.dot(moe_in, shared_up, preferred_element_type=jnp.float32)
    ).astype(jnp.bfloat16)
    shared_out = jnp.dot(shared_hidden, shared_down, preferred_element_type=jnp.float32)
    layer_out = (after_mixer.astype(jnp.float32) + routed + shared_out).astype(jnp.bfloat16)
    return (layer_out, key_new.reshape(tok_dev, -1), value_new)


def solution(mesh):
    torus = Mesh(mesh.devices.reshape(4, 4, 4, 2), ("ep_0", "ep_1", "ep_2", "ep_3"))
    return jax.shard_map(
        on_device,
        mesh=torus,
        in_specs=(
            P(EP, None),
            P(EP),
            P(EP, None, None),
            P(EP, None, None),
            P(EP, None),
            P(EP, None),
            P(EP, None),
            P(EP, None),
            P(),
            P(),
            P(),
            P(),
            P(),
            P(),
            P(EP, None, None),
            P(EP, None, None),
            P(EP, None, None),
            P(),
            P(),
            P(),
        ),
        out_specs=(P(EP, None), P(EP, None), P(EP, None)),
        check_vma=False,
    )
```

profile of v0, /device:TPU:1, one launch (start us, length us, event | category | flops | bytes accessed | tf_op | source)
XLA Modules:
  0.0 221.3 jit_solution(17257553948698546519)
XLA Ops:
  7.2 0.7 all-gather.3.cloned.1.call-update
  7.9 0.9 pad_maximum_fusion
  8.8 0.8 all_to_all.52
  9.6 0.3 copy.126
  10.0 1.2 reshape.270
  11.2 11.5 %all-to-all-start = ((bf16[128,2,192]{2,1,0:T(2,128)(2,1)}), bf16[128,2,192]{2,1,0:T(2,128)(2,1)S(1)}, u32[]{:S(2)}, u32[]{:S(2)}) async-start(bf16[128,2,192]{2,1,0:T(2,128)(2,1)} %reshape.270), calls=%async_computation | async-start | bytes 262144 | tf_op jit(solution)/shard_map/all_to_all | solution.py:145
  22.8 9.9 %all-to-all-done = bf16[128,2,192]{2,1,0:T(2,128)(2,1)S(1)} async-done(((bf16[128,2,192]{2,1,0:T(2,128)(2,1)}), bf16[128,2,192]{2,1,0:T(2,128)(2,1)S(1)}, u32[]{:S(2)}, u32[]{:S(2)}) %all-to-all-start) | async-done | bytes 98336 | tf_op jit(solution)/shard_map/all_to_all | solution.py:145
  32.7 1.2 reshape.271
  33.9 44.1 %all-gather.3.cloned.1.call-done = bf16[128,2,2048]{2,1,0:T(2,128)(2,1)} async-done(((bf16[1,2,2048]{2,1,0:T(2,128)(2,1)}), bf16[128,2,2048]{2,1,0:T(2,128)(2,1)}) %all-gather.3.cloned.1.call-update) | async-done | bytes 1048592 | tf_op jit(solution)/shard_map/all_gather | solution.py:142
  78.0 2.5 %reshape.265 = f32[256,2048]{1,0:T(8,128)} reshape(bf16[128,2,2048]{2,1,0:T(2,128)(2,1)} %all-gather.3.cloned.1.call-done) | data formatting | bytes 3145728 | tf_op jit(solution)/shard_map/convert_element_type | solution.py:39
  80.6 2.0 multiply_reduce_fusion.1
  82.5 0.2 copy-done.1
  82.8 0.2 multiply_convert_fusion
  83.0 1.5 dot_general.41
  84.5 2.1 fusion.29
  86.6 0.8 copy.77
  87.4 5.4 %all-to-all-start.1 = ((f32[128,2,24]{2,1,0:T(2,128)}), f32[128,2,24]{2,1,0:T(2,128)S(1)}, u32[]{:S(2)}, u32[]{:S(2)}) async-start(f32[128,2,24]{2,1,0:T(2,128)} %copy.77), calls=%async_computation.1 | async-start | bytes 262144 | tf_op jit(solution)/shard_map/all_to_all | solution.py:147
  92.7 0.1 multiply_cosine_fusion
  92.9 4.0 %reshape.254 = bf16[2,1024,2,2,128]{4,3,2,1,0:T(2,128)(2,1)} reshape(bf16[2,1024,512]{2,1,0:T(8,128)(2,1)} %param.22) | data formatting | bytes 4194304 | tf_op jit(solution)/shard_map/reshape | solution.py:66
  96.8 0.1 mul.265
  96.9 5.8 %all-to-all-done.1 = f32[128,2,24]{2,1,0:T(2,128)S(1)} async-done(((f32[128,2,24]{2,1,0:T(2,128)}), f32[128,2,24]{2,1,0:T(2,128)S(1)}, u32[]{:S(2)}, u32[]{:S(2)}) %all-to-all-start.1) | async-done | bytes 24608 | tf_op jit(solution)/shard_map/all_to_all | solution.py:147
  102.8 0.1 all_to_all.58
  103.0 0.1 fusion.61
  103.1 0.1 fusion.75
  103.3 0.2 fusion.52
  103.5 2.4 %select_reduce_fusion = (f32[2,2,4,2]{2,3,1,0:T(2,128)S(1)}, f32[2,2,4,2,1024]{4,2,3,1,0:T(4,128)S(1)}) fusion(pred[2,1024]{1,0:T(4,128)(4,1)S(1)} %iota_compare_fusion.1, bf16[2,1024,2,2,128]{4,3,2,1,0:T(2,128)(2,1)} %reshape.254, bf16[2,2,4,2,64]{4,2,3,1,0:T(4,128)(2,1)S(1)} %get-tuple-element.8, bf16[2,2,4,2,64]{4,2,3,1,0:T(4,128)(2,1)S(1)} %get-tuple-element.7), kind=kOutput, calls=%fused_computation.31 | convolution fusion | flops 8503264 | bytes 2238592 | tf_op jit(solution)/shard_map/skgph,sckph->skgpc/dot_general | solution.py:71
  105.8 0.2 fusion.60
  106.1 2.1 multiply_reduce_fusion.2
  108.2 0.1 multiply_convert_fusion.1
  108.3 0.1 all_to_all.59
  108.5 13.7 %all_to_all.74 = bf16[2,128,16]{2,0,1:T(2,128)(2,1)S(1)} all-to-all(bf16[2,128,16]{2,0,1:T(2,128)(2,1)S(1)} %copy.84), channel_id=1, replica_groups=mesh['ep_0'=4,'ep_1'=4,'ep_2'=4,'ep_3'=2] {'ep_0','ep_1','ep_2','ep_3'}, dimensions={1} | all-to-all | bytes 16384 | tf_op jit(solution)/shard_map/all_to_all | solution.py:162
  122.2 0.4 convolution_convert_fusion.1
  122.6 1.5 reshape_reshape.3
  124.1 1.9 copy.125
  126.0 5.0 %all_to_all.75 = bf16[2,64,2,2048]{3,2,1,0:T(2,128)(2,1)S(1)} all-to-all(bf16[2,64,2,2048]{3,2,1,0:T(2,128)(2,1)S(1)} %bitcast.97), channel_id=1, replica_groups=mesh['ep_0'=4,'ep_1'=4,'ep_2'=4,'ep_3'=2] {'ep_3'}, dimensions={0} | all-to-all | bytes 2097152 | tf_op jit(solution)/shard_map/all_to_all | solution.py:24
  131.0 3.1 %reduce_sum.90 = bf16[64,2,2048]{2,1,0:T(2,128)(2,1)} reduce(bf16[2,64,2,2048]{3,2,1,0:T(2,128)(2,1)S(1)} %all_to_all.75, bf16[]{:T(256)} %constant.30.clone.1), dimensions={0}, to_apply=%region_4.5 | reduce | flops 262144 | bytes 1572866 | tf_op jit(solution)/shard_map/reduce_sum | solution.py:25
  134.1 4.9 %all-to-all-start.4 = ((bf16[64,2,2048]{2,1,0:T(2,128)(2,1)}), bf16[64,2,2048]{2,1,0:T(2,128)(2,1)S(1)}, u32[]{:S(2)}, u32[]{:S(2)}) async-start(bf16[64,2,2048]{2,1,0:T(2,128)(2,1)} %reduce_sum.90), calls=%async_computation.4 | async-start | bytes 1048576 | tf_op jit(solution)/shard_map/all_to_all | solution.py:32
  139.1 0.1 fusion.47
  139.2 0.1 copy.88
  139.3 12.1 %all-to-all-done.4 = bf16[64,2,2048]{2,1,0:T(2,128)(2,1)S(1)} async-done(((bf16[64,2,2048]{2,1,0:T(2,128)(2,1)}), bf16[64,2,2048]{2,1,0:T(2,128)(2,1)S(1)}, u32[]{:S(2)}, u32[]{:S(2)}) %all-to-all-start.4) | async-done | bytes 524320 | tf_op jit(solution)/shard_map/all_to_all | solution.py:32
  151.4 0.4 reduce_sum.91
  151.9 0.1 fusion.40
  152.0 0.1 fusion.42
  152.1 1.8 broadcast_select_fusion
  153.9 5.3 %all-to-all-start.5 = ((bf16[128,2,2048]{2,1,0:T(2,128)(2,1)}), bf16[128,2,2048]{2,1,0:T(2,128)(2,1)S(1)}, u32[]{:S(2)}, u32[]{:S(2)}) async-start(bf16[128,2,2048]{2,1,0:T(2,128)(2,1)} %broadcast_select_fusion), calls=%async_computation.5 | async-start | bytes 2097152 | tf_op jit(solution)/shard_map/all_to_all | solution.py:180
  159.2 0.3 reduce-window.9
  159.6 0.1 slice_reduce_fusion
  159.8 18.7 %all-to-all-done.5 = bf16[128,2,2048]{2,1,0:T(2,128)(2,1)S(1)} async-done(((bf16[128,2,2048]{2,1,0:T(2,128)(2,1)}), bf16[128,2,2048]{2,1,0:T(2,128)(2,1)S(1)}, u32[]{:S(2)}, u32[]{:S(2)}) %all-to-all-start.5) | async-done | bytes 1048608 | tf_op jit(solution)/shard_map/all_to_all | solution.py:180
  178.6 1.2 reshape.259
  179.8 1.6 convolution_convert_fusion.3
  181.4 2.0 fusion.7
  183.4 0.4 fusion.22
  183.8 0.7 convolution_convert_fusion
  184.5 1.5 reshape.260
  186.0 4.4 %all-to-all-start.6 = ((bf16[128,2,2048]{2,1,0:T(2,128)(2,1)}), bf16[128,2,2048]{2,1,0:T(2,128)(2,1)S(1)}, u32[]{:S(2)}, u32[]{:S(2)}) async-start(bf16[128,2,2048]{2,1,0:T(2,128)(2,1)} %reshape.260), calls=%async_computation.6 | async-start | bytes 2097152 | tf_op jit(solution)/shard_map/all_to_all | solution.py:184
  190.5 0.1 constant_dynamic-slice_fusion
  190.5 0.1 select_reduce_fusion.1
  190.6 0.1 copy.89
  190.8 0.1 maximum_convert_fusion
  190.8 0.6 convert_element_type.114
  191.4 2.0 fusion.62
  193.4 16.4 %all-to-all-done.6 = bf16[128,2,2048]{2,1,0:T(2,128)(2,1)S(1)} async-done(((bf16[128,2,2048]{2,1,0:T(2,128)(2,1)}), bf16[128,2,2048]{2,1,0:T(2,128)(2,1)S(1)}, u32[]{:S(2)}, u32[]{:S(2)}) %all-to-all-start.6) | async-done | bytes 1048608 | tf_op jit(solution)/shard_map/all_to_all | solution.py:184
  209.8 1.1 multiply_reduce_fusion
  210.9 3.6 %fusion = bf16[2,2048]{1,0:T(2,128)(2,1)} fusion(bf16[512,2048]{1,0:T(8,128)(2,1)} %param.39, bf16[2,2048]{1,0:T(2,128)(2,1)S(1)} %fusion.42, bf16[2048,512]{1,0:T(8,128)(2,1)} %param.38, f32[2,2048]{1,0:T(2,128)S(1)} %multiply_reduce_fusion, f32[2,512]{1,0:T(2,128)S(1)} %fusion.62, bf16[2,2048]{1,0:T(2,128)(2,1)S(1)} %reduce_sum.91, ...), kind=kOutput, calls=%fused_computation.5 | convolution fusion | flops 8427520 | bytes 4247552 | tf_op jit(solution)/shard_map/dot_general | solution.py:192
  (51 shorter events, 0.8 us)
Async XLA Ops:
  7.2 176.6 %copy-start = (bf16[1,512,2048]{2,1,0:T(8,128)(2,1)S(1)}, bf16[1,512,2048]{2,1,0:T(8,128)(2,1)}, u32[]{:S(2)}) copy-start(bf16[1,512,2048]{2,1,0:T(8,128)(2,1)} %param.36) | copy-start | bytes 6291460
  7.2 15.5 %copy-start.11 = (s32[2]{0:T(128)S(1)}, s32[2]{0:T(128)}, u32[]{:S(2)}) copy-start(s32[2]{0:T(128)} %param.21) | copy-start | bytes 28
  7.2 70.8 %all-gather.3.cloned.1.call-start = ((), (), s32[]{:S(2)}) async-start(), calls=%async_computation.7 | async-start | bytes 1056768 | tf_op jit(solution)/shard_map/all_gather | solution.py:142
  11.2 21.5 %all-to-all-start = ((bf16[128,2,192]{2,1,0:T(2,128)(2,1)}), bf16[128,2,192]{2,1,0:T(2,128)(2,1)S(1)}, u32[]{:S(2)}, u32[]{:S(2)}) async-start(bf16[128,2,192]{2,1,0:T(2,128)(2,1)} %reshape.270), calls=%async_computation | async-start | bytes 262144 | tf_op jit(solution)/shard_map/all_to_all | solution.py:145
  33.9 48.7 %copy-start.6 = (f32[2048]{0:T(1024)S(1)}, f32[2048]{0:T(1024)}, u32[]{:S(2)}) copy-start(f32[2048]{0:T(1024)} %param.30) | copy-start | bytes 24580
  80.6 2.2 %copy-start.1 = (f32[256,2048]{1,0:T(8,128)S(1)}, f32[256,2048]{1,0:T(8,128)}, u32[]{:S(2)}) copy-start(f32[256,2048]{1,0:T(8,128)} %reshape.265) | copy-start | bytes 6291460
  87.4 15.4 %all-to-all-start.1 = ((f32[128,2,24]{2,1,0:T(2,128)}), f32[128,2,24]{2,1,0:T(2,128)S(1)}, u32[]{:S(2)}, u32[]{:S(2)}) async-start(f32[128,2,24]{2,1,0:T(2,128)} %copy.77), calls=%async_computation.1 | async-start | bytes 262144 | tf_op jit(solution)/shard_map/all_to_all | solution.py:147
  92.9 4.0 %copy-start.12 = (f32[8]{0:T(128)S(1)}, f32[8]{0:T(128)}, u32[]{:S(2)}) copy-start(f32[8]{0:T(128)} %param.28) | copy-start | bytes 100
  102.9 5.3 %copy-start.7 = (bf16[2,512]{1,0:T(2,128)(2,1)}, bf16[2,512]{1,0:T(2,128)(2,1)S(1)}, u32[]{:S(2)}) copy-start(bf16[2,512]{1,0:T(2,128)(2,1)S(1)} %slice.111) | copy-start | bytes 6148
  105.8 2.4 %copy-start.10 = (f32[256]{0:T(256)S(1)}, f32[256]{0:T(256)}, u32[]{:S(2)}) copy-start(f32[256]{0:T(256)} %param.29) | copy-start | bytes 3076
  105.8 16.3 %copy-start.4 = (bf16[16,2048]{1,0:T(8,128)(2,1)S(1)}, bf16[16,2048]{1,0:T(8,128)(2,1)}, u32[]{:S(2)}) copy-start(bf16[16,2048]{1,0:T(8,128)(2,1)} %param.27) | copy-start | bytes 196612
  126.0 13.0 %copy-start.5 = (s32[256,6]{0,1:T(8,128)S(1)}, s32[256,6]{0,1:T(8,128)}, u32[]{:S(2)}) copy-start(s32[256,6]{0,1:T(8,128)} %param.32) | copy-start | bytes 18436
  131.0 20.9 %copy-start.3 = (bf16[2,2048]{1,0:T(2,128)(2,1)S(1)}, bf16[2,2048]{1,0:T(2,128)(2,1)}, u32[]{:S(2)}) copy-start(bf16[2,2048]{1,0:T(2,128)(2,1)} %param.20) | copy-start | bytes 24580
  131.0 21.0 %copy-start.8 = (f32[2048]{0:T(1024)S(1)}, f32[2048]{0:T(1024)}, u32[]{:S(2)}) copy-start(f32[2048]{0:T(1024)} %param.31) | copy-start | bytes 24580
  134.1 17.3 %all-to-all-start.4 = ((bf16[64,2,2048]{2,1,0:T(2,128)(2,1)}), bf16[64,2,2048]{2,1,0:T(2,128)(2,1)S(1)}, u32[]{:S(2)}, u32[]{:S(2)}) async-start(bf16[64,2,2048]{2,1,0:T(2,128)(2,1)} %reduce_sum.90), calls=%async_computation.4 | async-start | bytes 1048576 | tf_op jit(solution)/shard_map/all_to_all | solution.py:32
  153.9 24.7 %all-to-all-start.5 = ((bf16[128,2,2048]{2,1,0:T(2,128)(2,1)}), bf16[128,2,2048]{2,1,0:T(2,128)(2,1)S(1)}, u32[]{:S(2)}, u32[]{:S(2)}) async-start(bf16[128,2,2048]{2,1,0:T(2,128)(2,1)} %broadcast_select_fusion), calls=%async_computation.5 | async-start | bytes 2097152 | tf_op jit(solution)/shard_map/all_to_all | solution.py:180
  179.8 3.6 %copy-start.2 = (bf16[1,2048,512]{2,1,0:T(8,128)(2,1)S(1)}, bf16[1,2048,512]{2,1,0:T(8,128)(2,1)}, u32[]{:S(2)}) copy-start(bf16[1,2048,512]{2,1,0:T(8,128)(2,1)} %param.35) | copy-start | bytes 6291460
  184.5 6.0 %copy-start.9 = (f32[256,6]{0,1:T(8,128)S(1)}, f32[256,6]{0,1:T(8,128)}, u32[]{:S(2)}) copy-start(f32[256,6]{0,1:T(8,128)} %param.33) | copy-start | bytes 18436
  186.0 23.8 %all-to-all-start.6 = ((bf16[128,2,2048]{2,1,0:T(2,128)(2,1)}), bf16[128,2,2048]{2,1,0:T(2,128)(2,1)S(1)}, u32[]{:S(2)}, u32[]{:S(2)}) async-start(bf16[128,2,2048]{2,1,0:T(2,128)(2,1)} %reshape.260), calls=%async_computation.6 | async-start | bytes 2097152 | tf_op jit(solution)/shard_map/all_to_all | solution.py:184
Sparse Core Ops, SparseCore 0:
  10.8 67.1 all-gather.2
where the time goes:
time: 222 us; the launch traced here: 221 us
  waiting for transfers between devices  108 us (49%)
  starting transfers between devices  31.5 us (14%)
  local copies, waits for them, and re-layouts  20.6 us (9%)
  blocking collectives  18.6 us (8%)
  matrix products  17.3 us (8%)
  between operations  14.3 us (6%)
  other arithmetic  11.2 us (5%)
    all_gather x1, waiting for transfers between devices, on_device(): all_rows = lax.all_gather(hidden_in, EP, axis=0, tiled=True)  44.1 us
    all_to_all x1, waiting for transfers between devices, on_device(): lax.all_to_all(outgoing, EP, split_axis=0, concat_axis=0, tiled=True)  18.7 us
    all_to_all x1, waiting for transfers between devices, on_device(): lax.all_to_all(result.reshape(devices, tok_dev, model_width), EP, split_a...  16.4 us
    all_to_all x1, blocking collectives, on_device(): lax.all_to_all(attn_out, EP, split_axis=1, concat_axis=0, tiled=True)  13.7 us
    all_to_all x1, waiting for transfers between devices, summed_rows(): lax.all_to_all(nearer.astype(jnp.bfloat16), far, split_axis=0, concat_axi...  12.1 us
    all_to_all x1, starting transfers between devices, on_device(): lax.all_to_all(joined_rows, EP, split_axis=1, concat_axis=0, tiled=True)  11.5 us
    all_to_all x1, waiting for transfers between devices, on_device(): lax.all_to_all(joined_rows, EP, split_axis=1, concat_axis=0, tiled=True)  9.9 us
    all_to_all x1, waiting for transfers between devices, on_device(): lax.all_to_all(column_sums, EP, split_axis=0, concat_axis=1, tiled=True)  5.83 us
  transfers between devices with their start and end apart: 6, of which 6 were waited for; matrix products, arithmetic and copies ran while one was open for 5% of the time, Pallas kernels for 0%

commit v1 on v0

--- a/solution.py
+++ b/solution.py
@@ -139,7 +139,10 @@
     device = lax.axis_index(EP)
     tok_dev = hidden_in.shape[0]
     model_width = hidden_in.shape[1]
-    all_rows = lax.all_gather(hidden_in, EP, axis=0, tiled=True)
+    devices_2 = lax.axis_size(EP)
+    parts = jnp.stack([hidden_in for _ in range(devices_2)])
+    parts = lax.all_to_all(parts, EP, split_axis=0, concat_axis=0)
+    all_rows = jnp.concatenate(parts, axis=0)
     normed = rms_scale(all_rows, attn_gain, eps_norm).astype(jnp.bfloat16)
     joined_rows = jnp.concatenate([query_w, key_w, value_w], axis=1)
     column_block = lax.all_to_all(joined_rows, EP, split_axis=1, concat_axis=0, tiled=True)

time: 222 us -> 180 us (0.81)
  waiting for transfers between devices: 108 us -> 71.1 us
  blocking collectives: 18.6 us -> 40.1 us
  between operations: 14.3 us -> 0.95 us
  starting transfers between devices: 31.5 us -> 23.3 us
  local copies, waits for them, and re-layouts: 20.6 us -> 17.2 us
    all_gather x1 -> x0, waiting for transfers between devices: 44.1 us -> none  [on_device(): all_rows = lax.all_gather(hidden_in, EP, axis=0, tiled=True)]
    all_to_all x0 -> x1, blocking collectives: none -> 21.4 us  [on_device(): lax.all_to_all(joined_rows, EP, split_axis=1, concat_axis=0, tiled=True)]
    all_to_all x1, waiting for transfers between devices: 9.9 us -> 17.9 us  [on_device(): parts = lax.all_to_all(parts, EP, split_axis=0, concat_axis=0)]
    all_to_all x1, starting transfers between devices: 11.5 us -> 4.32 us  [on_device(): parts = lax.all_to_all(parts, EP, split_axis=0, concat_axis=0)]
    convert_element_type x1 -> x0, local copies, waits for them, and re-layouts: 2.54 us -> none  [rms_scale(): row_block = row_block.astype(jnp.float32)]
  transfers between devices with their start and end apart: 6 -> 5, of which waited for: 6 -> 5; matrix products, arithmetic and copies ran while one was open for 5% -> 5% of each run, Pallas kernels for 0% -> 0%
where the time goes in v1:
time: 180 us; the launch traced here: 179 us
  waiting for transfers between devices  71.1 us (39%)
  blocking collectives  40.1 us (22%)
  starting transfers between devices  23.3 us (13%)
  local copies, waits for them, and re-layouts  17.2 us (10%)
  matrix products  17.1 us (10%)
  other arithmetic  9.54 us (5%)
    all_to_all x1, blocking collectives, on_device(): lax.all_to_all(joined_rows, EP, split_axis=1, concat_axis=0, tiled=True)  21.4 us
    all_to_all x1, waiting for transfers between devices, on_device(): lax.all_to_all(outgoing, EP, split_axis=0, concat_axis=0, tiled=True)  18.7 us
    all_to_all x1, waiting for transfers between devices, on_device(): parts = lax.all_to_all(parts, EP, split_axis=0, concat_axis=0)  17.9 us
    all_to_all x1, waiting for transfers between devices, on_device(): lax.all_to_all(result.reshape(devices, tok_dev, model_width), EP, split_a...  16.4 us
    all_to_all x1, blocking collectives, on_device(): lax.all_to_all(attn_out, EP, split_axis=1, concat_axis=0, tiled=True)  13.7 us
    all_to_all x1, waiting for transfers between devices, summed_rows(): lax.all_to_all(nearer.astype(jnp.bfloat16), far, split_axis=0, concat_axi...  12.2 us
    all_to_all x1, waiting for transfers between devices, on_device(): lax.all_to_all(column_sums, EP, split_axis=0, concat_axis=1, tiled=True)  5.92 us
    all_to_all x1, starting transfers between devices, on_device(): lax.all_to_all(outgoing, EP, split_axis=0, concat_axis=0, tiled=True)  5.21 us
  transfers between devices with their start and end apart: 5, of which 5 were waited for; matrix products, arithmetic and copies ran while one was open for 5% of the time, Pallas kernels for 0%

profile of v1, /device:TPU:1, one launch (start us, length us, event | category | flops | bytes accessed | tf_op | source)
XLA Modules:
  0.0 179.2 jit_solution(14020904073159830725)
XLA Ops:
  0.7 1.0 pad_maximum_fusion
  1.7 0.8 all_to_all.56
  2.5 0.3 copy.144
  2.9 0.5 reshape.283
  3.4 21.4 %all_to_all.79 = bf16[128,2,192]{2,1,0:T(2,128)(2,1)S(1)} all-to-all(bf16[128,2,192]{2,1,0:T(2,128)(2,1)S(1)} %reshape.283), channel_id=1, replica_groups=mesh['ep_0'=4,'ep_1'=4,'ep_2'=4,'ep_3'=2] {'ep_0','ep_1','ep_2','ep_3'}, dimensions={0} | all-to-all | bytes 196608 | tf_op jit(solution)/shard_map/all_to_all | solution.py:148
  24.9 1.5 stack.2
  26.4 4.3 %all-to-all-start = ((bf16[128,2,2048]{2,1,0:T(2,128)(2,1)}), bf16[128,2,2048]{2,1,0:T(2,128)(2,1)S(1)}, u32[]{:S(2)}, u32[]{:S(2)}) async-start(bf16[128,2,2048]{2,1,0:T(2,128)(2,1)} %stack.2), calls=%async_computation | async-start | bytes 2097152 | tf_op jit(solution)/shard_map/all_to_all | solution.py:144
  30.8 0.1 iota_compare_fusion.1
  30.8 1.2 reshape.284
  32.1 17.9 %all-to-all-done = bf16[128,2,2048]{2,1,0:T(2,128)(2,1)S(1)} async-done(((bf16[128,2,2048]{2,1,0:T(2,128)(2,1)}), bf16[128,2,2048]{2,1,0:T(2,128)(2,1)S(1)}, u32[]{:S(2)}, u32[]{:S(2)}) %all-to-all-start) | async-done | bytes 1048608 | tf_op jit(solution)/shard_map/all_to_all | solution.py:144
  50.0 0.4 fusion.1
  50.4 1.8 fusion.32
  52.1 0.8 copy.92
  52.9 4.4 %all-to-all-start.2 = ((f32[128,2,24]{2,1,0:T(2,128)}), f32[128,2,24]{2,1,0:T(2,128)S(1)}, u32[]{:S(2)}, u32[]{:S(2)}) async-start(f32[128,2,24]{2,1,0:T(2,128)} %copy.92), calls=%async_computation.2 | async-start | bytes 262144 | tf_op jit(solution)/shard_map/all_to_all | solution.py:150
  57.3 0.1 multiply_cosine_fusion
  57.5 4.0 %reshape.270 = bf16[2,1024,2,2,128]{4,3,2,1,0:T(2,128)(2,1)} reshape(bf16[2,1024,512]{2,1,0:T(8,128)(2,1)} %param.22) | data formatting | bytes 4194304 | tf_op jit(solution)/shard_map/reshape | solution.py:66
  61.4 0.1 mul.268
  61.5 5.9 %all-to-all-done.2 = f32[128,2,24]{2,1,0:T(2,128)S(1)} async-done(((f32[128,2,24]{2,1,0:T(2,128)}), f32[128,2,24]{2,1,0:T(2,128)S(1)}, u32[]{:S(2)}, u32[]{:S(2)}) %all-to-all-start.2) | async-done | bytes 24608 | tf_op jit(solution)/shard_map/all_to_all | solution.py:150
  67.5 0.1 all_to_all.62
  67.7 0.1 fusion.67
  67.8 0.1 multiply_subtract_fusion
  67.8 0.1 fusion.81
  67.9 0.2 fusion.58
  68.1 2.4 %select_reduce_fusion = (f32[2,2,4,2]{2,3,1,0:T(2,128)S(1)}, f32[2,2,4,2,1024]{4,2,3,1,0:T(4,128)S(1)}) fusion(pred[2,1024]{1,0:T(4,128)(4,1)S(1)} %iota_compare_fusion.1, bf16[2,1024,2,2,128]{4,3,2,1,0:T(2,128)(2,1)} %reshape.270, bf16[2,2,4,2,64]{4,2,3,1,0:T(4,128)(2,1)S(1)} %get-tuple-element.8, bf16[2,2,4,2,64]{4,2,3,1,0:T(4,128)(2,1)S(1)} %get-tuple-element.7), kind=kOutput, calls=%fused_computation.36 | convolution fusion | flops 8503264 | bytes 2238592 | tf_op jit(solution)/shard_map/skgph,sckph->skgpc/dot_general | solution.py:71
  70.5 0.2 fusion.66
  70.8 2.1 %multiply_reduce_fusion.1 = (f32[2,2,4]{2,1,0:T(2,128)S(1)}, f32[2,2,4,256]{3,2,1,0:T(4,128)S(1)}) fusion(f32[2,2,256]{2,1,0:T(2,128)S(1)} %reshape.278, f32[2,2,4]{2,1,0:T(2,128)S(1)} %bitcast.105, bf16[2,128,2,8,256]{4,3,2,1,0:T(8,128)(2,1)} %bitcast.109, f32[2,2,4,2,1024]{4,2,3,1,0:T(4,128)S(1)} %get-tuple-element.6, f32[2,2,4]{2,1,0:T(2,128)S(1)} %bitcast.106, ...), kind=kOutput, calls=%fused_computation.56 | convolution fusion | flops 8486896 | bytes 2248992 | tf_op jit(solution)/shard_map/skgc,sckv->skgv/dot_general | solution.py:91
  72.9 0.1 multiply_convert_fusion
  73.0 0.1 all_to_all.63
  73.2 13.7 %all_to_all.80 = bf16[2,128,16]{2,0,1:T(2,128)(2,1)S(1)} all-to-all(bf16[2,128,16]{2,0,1:T(2,128)(2,1)S(1)} %copy.99), channel_id=1, replica_groups=mesh['ep_0'=4,'ep_1'=4,'ep_2'=4,'ep_3'=2] {'ep_0','ep_1','ep_2','ep_3'}, dimensions={1} | all-to-all | bytes 16384 | tf_op jit(solution)/shard_map/all_to_all | solution.py:165
  86.8 0.4 convolution_convert_fusion.1
  87.2 1.5 reshape_reshape.3
  88.8 1.9 %copy.143 = bf16[64,2,2,2048]{3,2,0,1:T(2,128)(2,1)S(1)} copy(bf16[64,2,2,2048]{3,2,1,0:T(2,128)(2,1)} %reshape_reshape.3) | data formatting | bytes 2097152 | tf_op jit(solution)/shard_map/reshape;reshape | solution.py:18
  90.7 5.0 %all_to_all.81 = bf16[2,64,2,2048]{3,2,1,0:T(2,128)(2,1)S(1)} all-to-all(bf16[2,64,2,2048]{3,2,1,0:T(2,128)(2,1)S(1)} %bitcast.96), channel_id=1, replica_groups=mesh['ep_0'=4,'ep_1'=4,'ep_2'=4,'ep_3'=2] {'ep_3'}, dimensions={0} | all-to-all | bytes 2097152 | tf_op jit(solution)/shard_map/all_to_all | solution.py:24
  95.7 3.1 %reduce_sum.90 = bf16[64,2,2048]{2,1,0:T(2,128)(2,1)} reduce(bf16[2,64,2,2048]{3,2,1,0:T(2,128)(2,1)S(1)} %all_to_all.81, bf16[]{:T(256)} %constant.30.clone.1), dimensions={0}, to_apply=%region_4.5 | reduce | flops 262144 | bytes 1572866 | tf_op jit(solution)/shard_map/reduce_sum | solution.py:25
  98.8 4.9 %all-to-all-start.5 = ((bf16[64,2,2048]{2,1,0:T(2,128)(2,1)}), bf16[64,2,2048]{2,1,0:T(2,128)(2,1)S(1)}, u32[]{:S(2)}, u32[]{:S(2)}) async-start(bf16[64,2,2048]{2,1,0:T(2,128)(2,1)} %reduce_sum.90), calls=%async_computation.5 | async-start | bytes 1048576 | tf_op jit(solution)/shard_map/all_to_all | solution.py:32
  103.7 0.1 constant_dynamic-slice_fusion.1
  103.8 0.1 fusion.53
  103.9 0.1 copy.103
  104.0 12.2 %all-to-all-done.5 = bf16[64,2,2048]{2,1,0:T(2,128)(2,1)S(1)} async-done(((bf16[64,2,2048]{2,1,0:T(2,128)(2,1)}), bf16[64,2,2048]{2,1,0:T(2,128)(2,1)S(1)}, u32[]{:S(2)}, u32[]{:S(2)}) %all-to-all-start.5) | async-done | bytes 524320 | tf_op jit(solution)/shard_map/all_to_all | solution.py:32
  116.2 0.4 reduce_sum.91
  116.7 0.1 fusion.46
  116.8 0.1 fusion.48
  116.9 1.8 %broadcast_select_fusion = bf16[128,2,2048]{2,1,0:T(2,128)(2,1)} fusion(pred[128,2]{1,0:T(8,128)(4,1)S(1)} %copy.103, bf16[2,2048]{1,0:T(2,128)(2,1)S(1)} %fusion.48), kind=kLoop, calls=%fused_computation.22 | loop fusion | flops 524288 | bytes 1057024 | tf_op jit(solution)/shard_map/jit(_where)/select_n | solution.py:182
  118.7 5.2 %all-to-all-start.6 = ((bf16[128,2,2048]{2,1,0:T(2,128)(2,1)}), bf16[128,2,2048]{2,1,0:T(2,128)(2,1)S(1)}, u32[]{:S(2)}, u32[]{:S(2)}) async-start(bf16[128,2,2048]{2,1,0:T(2,128)(2,1)} %broadcast_select_fusion), calls=%async_computation.6 | async-start | bytes 2097152 | tf_op jit(solution)/shard_map/all_to_all | solution.py:183
  124.0 0.3 reduce-window.9
  124.3 0.1 slice.62
  124.4 0.1 slice_reduce_fusion
  124.6 18.7 %all-to-all-done.6 = bf16[128,2,2048]{2,1,0:T(2,128)(2,1)S(1)} async-done(((bf16[128,2,2048]{2,1,0:T(2,128)(2,1)}), bf16[128,2,2048]{2,1,0:T(2,128)(2,1)S(1)}, u32[]{:S(2)}, u32[]{:S(2)}) %all-to-all-start.6) | async-done | bytes 1048608 | tf_op jit(solution)/shard_map/all_to_all | solution.py:183
  143.3 1.2 reshape.275
  144.5 1.6 convolution_convert_fusion.3
  146.1 2.0 %fusion.10 = f32[24,512]{1,0:T(8,128)S(1)} fusion(bf16[24,2048]{1,0:T(8,128)(2,1)S(1)} %convolution_convert_fusion.3, bf16[1,2048,512]{2,1,0:T(8,128)(2,1)} %param.34), kind=kOutput, calls=%fused_computation.17 | convolution fusion | flops 50331648 | bytes 2244608 | tf_op jit(solution)/shard_map/dot_general | solution.py:109
  148.1 0.4 fusion.25
  148.5 0.7 convolution_convert_fusion
  149.2 1.5 reshape.276
  150.8 4.4 %all-to-all-start.7 = ((bf16[128,2,2048]{2,1,0:T(2,128)(2,1)}), bf16[128,2,2048]{2,1,0:T(2,128)(2,1)S(1)}, u32[]{:S(2)}, u32[]{:S(2)}) async-start(bf16[128,2,2048]{2,1,0:T(2,128)(2,1)} %reshape.276), calls=%async_computation.7 | async-start | bytes 2097152 | tf_op jit(solution)/shard_map/all_to_all | solution.py:187
  155.2 0.1 constant_dynamic-slice_fusion
  155.3 0.1 select_reduce_fusion.1
  155.4 0.1 copy.104
  155.5 0.1 maximum_convert_fusion
  155.6 0.6 convert_element_type.117
  156.2 2.0 %fusion.68 = f32[2,512]{1,0:T(2,128)S(1)} fusion(bf16[2,2048]{1,0:T(2,128)(2,1)S(1)} %fusion.48, bf16[2048,512]{1,0:T(8,128)(2,1)} %param.37), kind=kOutput, calls=%fused_computation.104 | convolution fusion | flops 4194304 | bytes 2109440 | tf_op jit(solution)/shard_map/dot_general | solution.py:192
  158.1 16.4 %all-to-all-done.7 = bf16[128,2,2048]{2,1,0:T(2,128)(2,1)S(1)} async-done(((bf16[128,2,2048]{2,1,0:T(2,128)(2,1)}), bf16[128,2,2048]{2,1,0:T(2,128)(2,1)S(1)}, u32[]{:S(2)}, u32[]{:S(2)}) %all-to-all-start.7) | async-done | bytes 1048608 | tf_op jit(solution)/shard_map/all_to_all | solution.py:187
  174.5 1.1 multiply_reduce_fusion
  175.7 3.6 %fusion = bf16[2,2048]{1,0:T(2,128)(2,1)} fusion(bf16[512,2048]{1,0:T(8,128)(2,1)} %param.39, bf16[2,2048]{1,0:T(2,128)(2,1)S(1)} %fusion.48, bf16[2048,512]{1,0:T(8,128)(2,1)} %param.38, f32[2,2048]{1,0:T(2,128)S(1)} %multiply_reduce_fusion, f32[2,512]{1,0:T(2,128)S(1)} %fusion.68, bf16[2,2048]{1,0:T(2,128)(2,1)S(1)} %reduce_sum.91, ...), kind=kOutput, calls=%fused_computation.7 | convolution fusion | flops 8427520 | bytes 4247552 | tf_op jit(solution)/shard_map/dot_general | solution.py:195
  (45 shorter events, 0.4 us)
Async XLA Ops:
  0.6 147.9 %copy-start = (bf16[1,512,2048]{2,1,0:T(8,128)(2,1)S(1)}, bf16[1,512,2048]{2,1,0:T(8,128)(2,1)}, u32[]{:S(2)}) copy-start(bf16[1,512,2048]{2,1,0:T(8,128)(2,1)} %param.36) | copy-start | bytes 6291460
  0.6 24.2 %copy-start.2 = (bf16[2,2048]{1,0:T(2,128)(2,1)S(1)}, bf16[2,2048]{1,0:T(2,128)(2,1)}, u32[]{:S(2)}) copy-start(bf16[2,2048]{1,0:T(2,128)(2,1)} %param.20) | copy-start | bytes 24580
  2.9 27.9 %copy-start.9 = (s32[2]{0:T(128)S(1)}, s32[2]{0:T(128)}, u32[]{:S(2)}) copy-start(s32[2]{0:T(128)} %param.21) | copy-start | bytes 28
  26.4 24.0 %copy-start.10 = (f32[2048]{0:T(1024)S(1)}, f32[2048]{0:T(1024)}, u32[]{:S(2)}) copy-start(f32[2048]{0:T(1024)} %param.30) | copy-start | bytes 24580
  26.4 23.6 %all-to-all-start = ((bf16[128,2,2048]{2,1,0:T(2,128)(2,1)}), bf16[128,2,2048]{2,1,0:T(2,128)(2,1)S(1)}, u32[]{:S(2)}, u32[]{:S(2)}) async-start(bf16[128,2,2048]{2,1,0:T(2,128)(2,1)} %stack.2), calls=%async_computation | async-start | bytes 2097152 | tf_op jit(solution)/shard_map/all_to_all | solution.py:144
  52.9 14.5 %all-to-all-start.2 = ((f32[128,2,24]{2,1,0:T(2,128)}), f32[128,2,24]{2,1,0:T(2,128)S(1)}, u32[]{:S(2)}, u32[]{:S(2)}) async-start(f32[128,2,24]{2,1,0:T(2,128)} %copy.92), calls=%async_computation.2 | async-start | bytes 262144 | tf_op jit(solution)/shard_map/all_to_all | solution.py:150
  57.5 4.0 %copy-start.11 = (f32[8]{0:T(128)S(1)}, f32[8]{0:T(128)}, u32[]{:S(2)}) copy-start(f32[8]{0:T(128)} %param.28) | copy-start | bytes 100
  67.6 5.3 %copy-start.5 = (bf16[2,512]{1,0:T(2,128)(2,1)}, bf16[2,512]{1,0:T(2,128)(2,1)S(1)}, u32[]{:S(2)}) copy-start(bf16[2,512]{1,0:T(2,128)(2,1)S(1)} %slice.111) | copy-start | bytes 6148
  70.5 2.4 %copy-start.8 = (f32[256]{0:T(256)S(1)}, f32[256]{0:T(256)}, u32[]{:S(2)}) copy-start(f32[256]{0:T(256)} %param.29) | copy-start | bytes 3076
  70.5 16.3 %copy-start.3 = (bf16[16,2048]{1,0:T(8,128)(2,1)S(1)}, bf16[16,2048]{1,0:T(8,128)(2,1)}, u32[]{:S(2)}) copy-start(bf16[16,2048]{1,0:T(8,128)(2,1)} %param.27) | copy-start | bytes 196612
  90.7 13.0 %copy-start.4 = (s32[256,6]{0,1:T(8,128)S(1)}, s32[256,6]{0,1:T(8,128)}, u32[]{:S(2)}) copy-start(s32[256,6]{0,1:T(8,128)} %param.32) | copy-start | bytes 18436
  95.7 21.1 %copy-start.6 = (f32[2048]{0:T(1024)S(1)}, f32[2048]{0:T(1024)}, u32[]{:S(2)}) copy-start(f32[2048]{0:T(1024)} %param.31) | copy-start | bytes 24580
  98.8 17.4 %all-to-all-start.5 = ((bf16[64,2,2048]{2,1,0:T(2,128)(2,1)}), bf16[64,2,2048]{2,1,0:T(2,128)(2,1)S(1)}, u32[]{:S(2)}, u32[]{:S(2)}) async-start(bf16[64,2,2048]{2,1,0:T(2,128)(2,1)} %reduce_sum.90), calls=%async_computation.5 | async-start | bytes 1048576 | tf_op jit(solution)/shard_map/all_to_all | solution.py:32
  118.7 24.6 %all-to-all-start.6 = ((bf16[128,2,2048]{2,1,0:T(2,128)(2,1)}), bf16[128,2,2048]{2,1,0:T(2,128)(2,1)S(1)}, u32[]{:S(2)}, u32[]{:S(2)}) async-start(bf16[128,2,2048]{2,1,0:T(2,128)(2,1)} %broadcast_select_fusion), calls=%async_computation.6 | async-start | bytes 2097152 | tf_op jit(solution)/shard_map/all_to_all | solution.py:183
  144.5 3.6 %copy-start.1 = (bf16[1,2048,512]{2,1,0:T(8,128)(2,1)S(1)}, bf16[1,2048,512]{2,1,0:T(8,128)(2,1)}, u32[]{:S(2)}) copy-start(bf16[1,2048,512]{2,1,0:T(8,128)(2,1)} %param.35) | copy-start | bytes 6291460
  149.2 6.0 %copy-start.7 = (f32[256,6]{0,1:T(8,128)S(1)}, f32[256,6]{0,1:T(8,128)}, u32[]{:S(2)}) copy-start(f32[256,6]{0,1:T(8,128)} %param.33) | copy-start | bytes 18436
  150.8 23.8 %all-to-all-start.7 = ((bf16[128,2,2048]{2,1,0:T(2,128)(2,1)}), bf16[128,2,2048]{2,1,0:T(2,128)(2,1)S(1)}, u32[]{:S(2)}, u32[]{:S(2)}) async-start(bf16[128,2,2048]{2,1,0:T(2,128)(2,1)} %reshape.276), calls=%async_computation.7 | async-start | bytes 2097152 | tf_op jit(solution)/shard_map/all_to_all | solution.py:187
